TPU v7x, 32 devices: a whole 2x2x4 slice. The times are simulated.
32 devices in a mesh: ep: 16 (over z, y, x), tp: 2 (over core).
Axes of the slice: x: 2, y: 2, z: 4, core: 2. Of those that a mesh axis runs over, the one named last changes fastest.
Arguments:
- tokens: bfloat16 [512, 2048], P('ep'), may hold values from -6 to 6
- mix_gain: float32 [2048], replicated, may hold values from 0.1 to 1.9
- w_query: bfloat16 [2048, 512], P('ep', 'tp'), may hold values from -0.125 to 0.125
- w_key: bfloat16 [2048, 512], P('ep', 'tp'), may hold values from -0.125 to 0.125
- w_value: bfloat16 [2048, 512], P('ep', 'tp'), may hold values from -0.125 to 0.125
- w_outgate: bfloat16 [2048, 512], P('ep', 'tp'), may hold values from -0.125 to 0.125
- w_igate: bfloat16 [2048, 8], P('ep', 'tp'), may hold values from -0.125 to 0.125
- w_fgate: bfloat16 [2048, 8], P('ep', 'tp'), may hold values from -0.125 to 0.125
- igate_bias: float32 [8], P('tp'), may hold values from -2 to 1
- fgate_bias: float32 [8], P('tp'), may hold values from 0 to 4
- head_gain: float32 [512], P('tp'), may hold values from 0.1 to 1.9
- w_out: bfloat16 [512, 2048], P('tp', 'ep'), may hold values from -0.25 to 0.25
- state_matrix: float32 [512, 8, 64, 64], P('ep', 'tp'), may hold values from -2.4 to 2.4
- state_norm: float32 [512, 8, 64], P('ep', 'tp'), may hold values from -2.4 to 2.4
- state_max: float32 [512, 8], P('ep', 'tp'), may hold values from -4 to 4
- ffn_gain: float32 [2048], replicated, may hold values from 0.1 to 1.9
- w_expert_gate: bfloat16 [16, 2048, 1408], P('ep', None, 'tp'), may hold values from -0.125 to 0.125
- w_expert_up: bfloat16 [16, 2048, 1408], P('ep', None, 'tp'), may hold values from -0.125 to 0.125
- w_expert_down: bfloat16 [16, 1408, 2048], P('ep', 'tp'), may hold values from -0.15625 to 0.15625
- routes: int32 [512, 3], P('ep'), may hold values from 0 to 15, all different within a row; in each aligned block of 32 rows (0 to 31, 32 to 63, ...) at most 12 rows name the same one
- route_weights: float32 [512, 3], P('ep'), may hold values from 0.2 to 1
Outputs:
- mixed: bfloat16 [512, 2048], P('ep')
- new_matrix: float32 [512, 8, 64, 64], P('ep', 'tp')
- new_norm: float32 [512, 8, 64], P('ep', 'tp')
- new_max: float32 [512, 8], P('ep', 'tp')
Inputs may be any that keep to these rules, and one draw needn't show every extreme that they name: `routes`: each row names 3 different experts. Among the rows of one device, no expert is named by more than 12 rows, a bound that some block reaches.
All inputs are finite; a program needn't handle non-finite values.
Results may differ from a plain program's by a relative error of at most 0.017.
Values may be sent and summed in bfloat16 or wider, within the bound.
No kernel may reach another device: no remote copies, remote signals or barrier semaphores. Data moves between devices by JAX's collectives and lax.ppermute only.
A program may use at most 128 MiB of HBM per device.

v0:
```python
import jax
import jax.numpy as jnp
from jax import lax
from jax.sharding import PartitionSpec as P


def rms_scale(values_in, gain_vec):
    widened = values_in.astype(jnp.float32)
    return (
        widened * lax.rsqrt(jnp.mean(widened * widened, axis=-1, keepdims=True) + 1e-06) * gain_vec
    )


def memory_cell(
    query,
    key_row,
    value_row,
    outgate,
    input_pre,
    forget_pre,
    head_gain,
    state_matrix,
    state_norm,
    state_max,
):
    seq_rows, head_count = input_pre.shape
    head_size = query.shape[1] // head_count
    query_heads = query.astype(jnp.float32).reshape(seq_rows, head_count, head_size)
    key_heads = key_row.astype(jnp.float32).reshape(
        seq_rows, head_count, head_size
    ) * head_size ** (-0.5)
    value_heads = value_row.astype(jnp.float32).reshape(seq_rows, head_count, head_size)
    log_forget = jax.nn.log_sigmoid(forget_pre)
    new_max = jnp.maximum(log_forget + state_max, input_pre)
    keep_old = jnp.exp(log_forget + state_max - new_max)
    keep_new = jnp.exp(input_pre - new_max)
    new_matrix = (
        keep_old[:, :, None, None] * state_matrix
        + keep_new[:, :, None, None] * value_heads[:, :, :, None] * key_heads[:, :, None, :]
    )
    new_norm = keep_old[:, :, None] * state_norm + keep_new[:, :, None] * key_heads
    numerator = jnp.sum(new_matrix * query_heads[:, :, None, :], axis=-1)
    denominator = jnp.sum(new_norm * query_heads, axis=-1)
    cell_read = numerator / jnp.maximum(jnp.abs(denominator), jnp.exp(-new_max))[:, :, None]
    centered = cell_read - jnp.mean(cell_read, axis=-1, keepdims=True)
    variance = jnp.mean(centered * centered, axis=-1, keepdims=True)
    scaled_cell = (centered * lax.rsqrt(variance + 1e-06)).reshape(seq_rows, head_count * head_size)
    cell_out = (scaled_cell * head_gain * jax.nn.sigmoid(outgate.astype(jnp.float32))).astype(
        jnp.bfloat16
    )
    return (cell_out, new_matrix, new_norm, new_max)


def torus_factors(count):
    side = 1
    while (2 * side) ** 3 <= count:
        side *= 2
    while count % (side * side):
        side -= 1
    return (count // (side * side), side, side)


def shift_pairs(factors, axis, step):
    pairs = []
    inner = 1
    for size in factors[axis + 1 :]:
        inner *= size
    total = factors[0] * factors[1] * factors[2]
    for source in range(total):
        place = source // inner % factors[axis]
        pairs.append((source, source + ((place + step) % factors[axis] - place) * inner))
    return pairs


def own_place(factors, axis):
    inner = 1
    for size in factors[axis + 1 :]:
        inner *= size
    return lax.axis_index("ep") // inner % factors[axis]


def reduce_stage(parts, factors, axis, dim):
    size = factors[axis]
    place = own_place(factors, axis)
    total = lax.dynamic_index_in_dim(parts, place, dim, keepdims=True).astype(jnp.float32)
    for step in range(1, size):
        sent = lax.dynamic_index_in_dim(parts, (place + step) % size, dim, keepdims=True)
        total = total + lax.ppermute(
            sent.astype(jnp.bfloat16), "ep", shift_pairs(factors, axis, step)
        ).astype(jnp.float32)
    return total


def staged_reduce_scatter(partial, factors, order):
    rows = partial.shape[0] // (factors[0] * factors[1] * factors[2])
    parts = partial.reshape(*factors, rows, partial.shape[1])
    for axis in order:
        parts = reduce_stage(parts, factors, axis, axis)
    return parts.reshape(rows, partial.shape[1])


def swap_cores(values_in):
    return lax.ppermute(values_in, "tp", [(0, 1), (1, 0)])


def body(
    tokens,
    mix_gain,
    w_query,
    w_key,
    w_value,
    w_outgate,
    w_igate,
    w_fgate,
    igate_bias,
    fgate_bias,
    head_gain,
    w_out,
    state_matrix,
    state_norm,
    state_max,
    ffn_gain,
    w_expert_gate,
    w_expert_up,
    w_expert_down,
    routes,
    route_weights,
):
    seq_rows, width = tokens.shape
    ep_count = lax.axis_size("ep")
    factors = torus_factors(ep_count)
    w_out_full = lax.all_gather(w_out, "ep", axis=1, tiled=True)
    local_experts = w_expert_gate.shape[0]
    expert_total = local_experts * ep_count
    top_count = routes.shape[1]
    capacity = max(2, 2 * seq_rows * top_count // expert_total)
    core_slots = -(-((capacity + 1) // 2) // 8) * 8
    core = lax.axis_index("tp")
    flat_routes = routes.reshape(-1)
    onehot = (flat_routes[:, None] == jnp.arange(expert_total, dtype=jnp.int32)[None, :]).astype(
        jnp.int32
    )
    earlier = jnp.cumsum(onehot, axis=0, dtype=jnp.int32) - onehot
    slots = jnp.sum(onehot * earlier, axis=1, dtype=jnp.int32)
    targets = jnp.where(slots % 2 == core, flat_routes * core_slots + slots // 2, -1)
    places = jnp.arange(expert_total * core_slots, dtype=jnp.int32)
    hits = (targets[:, None] == places[None, :]).reshape(seq_rows, top_count, -1)
    token_hits = jnp.any(hits, axis=1).astype(jnp.bfloat16)
    weight_hits = jnp.sum(jnp.where(hits, route_weights[:, :, None], 0.0), axis=1)
    normed = rms_scale(tokens, mix_gain).astype(jnp.bfloat16)
    spread = lax.all_to_all(normed, "ep", split_axis=1, concat_axis=0, tiled=True)
    first_list = (w_query, w_key)
    second_list = (w_value, w_outgate, w_igate, w_fgate)
    first = staged_reduce_scatter(
        jnp.dot(
            spread, jnp.concatenate(first_list, axis=1), preferred_element_type=jnp.float32
        ).astype(jnp.bfloat16),
        factors,
        (2, 1, 0),
    )
    second = staged_reduce_scatter(
        jnp.dot(
            spread, jnp.concatenate(second_list, axis=1), preferred_element_type=jnp.float32
        ).astype(jnp.bfloat16),
        factors,
        (1, 2, 0),
    )
    head_width = w_query.shape[1]
    head_count = w_igate.shape[1]
    query = first[:, :head_width].astype(jnp.bfloat16)
    key_row = first[:, head_width:].astype(jnp.bfloat16)
    value_row = second[:, :head_width].astype(jnp.bfloat16)
    outgate = second[:, head_width : 2 * head_width].astype(jnp.bfloat16)
    input_pre = second[:, 2 * head_width : 2 * head_width + head_count] + igate_bias
    forget_pre = second[:, 2 * head_width + head_count :] + fgate_bias
    cell_out, new_matrix, new_norm, new_max = memory_cell(
        query,
        key_row,
        value_row,
        outgate,
        input_pre,
        forget_pre,
        head_gain,
        state_matrix,
        state_norm,
        state_max,
    )
    partial_out = jnp.dot(cell_out, w_out_full, preferred_element_type=jnp.float32).astype(
        jnp.bfloat16
    )
    attended = partial_out.astype(jnp.float32) + swap_cores(partial_out).astype(jnp.float32)
    resid = (tokens.astype(jnp.float32) + attended).astype(jnp.bfloat16)
    normed_two = rms_scale(resid, ffn_gain).astype(jnp.bfloat16)
    outgoing = lax.dot_general(
        token_hits, normed_two, (((0,), (0,)), ((), ())), preferred_element_type=jnp.float32
    ).astype(jnp.bfloat16)
    outgoing = outgoing.reshape(expert_total, core_slots, width)
    received = lax.all_to_all(outgoing, "ep", split_axis=0, concat_axis=0, tiled=True)
    other = swap_cores(received)

    def grouped(rows):
        rows = rows.reshape(ep_count, local_experts, core_slots, width)
        return jnp.swapaxes(rows, 0, 1).reshape(local_experts, ep_count * core_slots, width)

    regrouped = jnp.concatenate([grouped(received), grouped(other)], axis=1)
    gate_pre = jnp.einsum(
        "xcd,xdf->xcf", regrouped, w_expert_gate, preferred_element_type=jnp.float32
    )
    up_pre = jnp.einsum("xcd,xdf->xcf", regrouped, w_expert_up, preferred_element_type=jnp.float32)
    hidden = (jax.nn.silu(gate_pre) * up_pre).astype(jnp.bfloat16)
    partial_down = jnp.einsum(
        "xcf,xfd->xcd", hidden, w_expert_down, preferred_element_type=jnp.float32
    ).astype(jnp.bfloat16)
    half = ep_count * core_slots
    expert_sum = (
        partial_down[:, :half].astype(jnp.float32)
        + swap_cores(partial_down[:, half:]).astype(jnp.float32)
    ).astype(jnp.bfloat16)
    finished = jnp.swapaxes(
        expert_sum.reshape(local_experts, ep_count, core_slots, width), 0, 1
    ).reshape(ep_count * local_experts, core_slots, width)
    returned = lax.all_to_all(finished, "ep", split_axis=0, concat_axis=0, tiled=True)
    returned = returned.reshape(expert_total * core_slots, width)
    weight_high = weight_hits.astype(jnp.bfloat16)
    weight_rest = weight_hits - weight_high.astype(jnp.float32)
    weight_low = weight_rest.astype(jnp.bfloat16)
    weighted = jnp.dot(weight_high, returned, preferred_element_type=jnp.float32) + jnp.dot(
        weight_low, returned, preferred_element_type=jnp.float32
    )
    weighted = weighted + swap_cores(weighted)
    mixed = (resid.astype(jnp.float32) + weighted).astype(jnp.bfloat16)
    return (mixed, new_matrix, new_norm, new_max)


def solution(mesh):
    placed = (
        P("ep", None),
        P(),
        P("ep", "tp"),
        P("ep", "tp"),
        P("ep", "tp"),
        P("ep", "tp"),
        P("ep", "tp"),
        P("ep", "tp"),
        P("tp"),
        P("tp"),
        P("tp"),
        P("tp", "ep"),
        P("ep", "tp", None, None),
        P("ep", "tp", None),
        P("ep", "tp"),
        P(),
        P("ep", None, "tp"),
        P("ep", None, "tp"),
        P("ep", "tp", None),
        P("ep", None),
        P("ep", None),
    )
    return jax.shard_map(
        body,
        mesh=mesh,
        in_specs=placed,
        out_specs=(P("ep", None), P("ep", "tp", None, None), P("ep", "tp", None), P("ep", "tp")),
        check_vma=False,
    )
```

profile of v0, /device:TPU:0, one launch (start us, length us, event | category | flops | bytes accessed | tf_op | source)
XLA Modules:
  0.0 143.0 jit_solution(14538455272105460633)
XLA Ops:
  7.2 0.7 all-gather.2.cloned.1.call-update
  7.9 1.2 fusion.29
  9.1 1.7 %copy_bitcast_fusion = bf16[32,16,128]{2,0,1:T(8,128)(2,1)} fusion(bf16[32,2048]{1,0:T(8,128)(2,1)} %param.21, f32[2048]{0:T(1024)} %param.22, f32[32]{0:T(128)S(1)} %add_rsqrt_fusion.2), kind=kLoop, calls=%fused_computation.56 | loop fusion | flops 262144 | bytes 270464 | tf_op jit(solution)/shard_map/all_to_all | solution.py:151
  10.8 8.3 %all-to-all-start = ((bf16[32,16,128]{2,0,1:T(8,128)(2,1)}), bf16[32,16,128]{2,0,1:T(8,128)(2,1)S(1)}, u32[]{:S(2)}, u32[]{:S(2)}) async-start(bf16[32,16,128]{2,0,1:T(8,128)(2,1)} %copy_bitcast_fusion), calls=%async_computation | async-start | bytes 262144 | tf_op jit(solution)/shard_map/all_to_all | solution.py:151
  19.2 1.4 copy.61
  20.6 0.8 copy.62
  21.5 0.8 copy.58
  22.3 0.8 copy.59
  23.2 0.1 reduce_window_sum.11
  23.3 0.2 select_reduce_fusion.1
  23.5 0.1 reduce_sum.80
  23.6 0.7 copy.63
  24.3 2.6 %all-to-all-done = bf16[32,16,128]{2,0,1:T(8,128)(2,1)S(1)} async-done(((bf16[32,16,128]{2,0,1:T(8,128)(2,1)}), bf16[32,16,128]{2,0,1:T(8,128)(2,1)S(1)}, u32[]{:S(2)}, u32[]{:S(2)}) %all-to-all-start) | async-done | bytes 131104 | tf_op jit(solution)/shard_map/all_to_all | solution.py:151
  26.9 1.2 convolution_convert_fusion.3
  28.1 0.8 constant_dynamic-slice_fusion
  28.9 1.1 collective-permute-start.5
  30.0 2.0 %convolution_convert_fusion.2 = bf16[512,520]{0,1:T(8,128)(2,1)} fusion(bf16[512,128]{1,0:T(8,128)(2,1)S(1)} %bitcast.61, bf16[128,4]{1,0:T(8,128)(2,1)S(1)} %copy.59, bf16[128,4]{1,0:T(8,128)(2,1)S(1)} %copy.58, bf16[128,256]{1,0:T(8,128)(2,1)} %param.26, bf16[128,256]{1,0:T(8,128)(2,1)} %param.25), kind=kOutput, calls=%fused_computation.14 | convolution fusion | flops 68956160 | bytes 796672 | tf_op jit(solution)/shard_map/dot_general | solution.py:162
  32.0 1.3 copy.60
  33.4 0.3 collective-permute-start
  33.6 2.2 %collective-permute-done.5 = bf16[4,2,1,32,512]{4,3,2,1,0:T(8,128)(2,1)} collective-permute-done((bf16[4,2,1,32,512]{4,3,2,1,0:T(8,128)(2,1)}, bf16[4,2,1,32,512]{4,3,2,1,0:T(8,128)(2,1)}, u32[]{:S(2)}, u32[]{:S(2)}) %collective-permute-start.5) | collective-permute-done | bytes 262176 | tf_op jit(solution)/shard_map/ppermute | solution.py:88
  35.8 1.1 convert_add_fusion.1
  36.9 1.0 collective-permute-start.6
  38.0 6.3 %collective-permute-done = bf16[4,1,2,32,520]{4,3,2,1,0:T(8,128)(2,1)S(1)} collective-permute-done((bf16[4,1,2,32,520]{4,3,2,1,0:T(8,128)(2,1)S(1)}, bf16[4,1,2,32,520]{4,3,2,1,0:T(8,128)(2,1)S(1)}, u32[]{:S(2)}, u32[]{:S(2)}) %collective-permute-start) | collective-permute-done | bytes 266272 | tf_op jit(solution)/shard_map/ppermute | solution.py:88
  44.4 0.7 collective-permute-start.1
  45.1 0.6 collective-permute-done.6
  45.8 0.4 collective-permute-start.7
  46.1 3.5 %collective-permute-start.9 = (bf16[1,1,1,32,512]{4,3,2,1,0:T(8,128)(2,1)S(1)}, bf16[1,1,1,32,512]{4,3,2,1,0:T(8,128)(2,1)S(1)}, u32[]{:S(2)}, u32[]{:S(2)}) collective-permute-start(bf16[1,1,1,32,512]{4,3,2,1,0:T(8,128)(2,1)S(1)} %get-tuple-element.33), channel_id=1, source_target_pairs={{0,24},{2,26},{4,28},{6,30},{8,0},{10,2},{12,4},{14,6},{16,8},{18,... | collective-permute-start | bytes 98312 | tf_op jit(solution)/shard_map/ppermute | solution.py:88
  49.6 0.1 collective-permute-done.1
  49.8 0.7 dynamic-slice_convert_fusion.4
  50.5 0.5 collective-permute-start.2
  51.0 3.3 %collective-permute-start.4 = (bf16[1,1,1,32,520]{4,3,2,1,0:T(8,128)(2,1)}, bf16[1,1,1,32,520]{4,3,2,1,0:T(8,128)(2,1)S(1)}, u32[]{:S(2)}, u32[]{:S(2)}) collective-permute-start(bf16[1,1,1,32,520]{4,3,2,1,0:T(8,128)(2,1)} %get-tuple-element.30), channel_id=1, source_target_pairs={{0,24},{2,26},{4,28},{6,30},{8,0},{10,2},{12,4},{14,6},{16,8},{18,... | collective-permute-start | bytes 99848 | tf_op jit(solution)/shard_map/ppermute | solution.py:88
  54.3 1.0 collective-permute-start.3
  55.5 1.7 %collective-permute-done.2 = bf16[1,1,1,32,520]{4,3,2,1,0:T(8,128)(2,1)S(1)} collective-permute-done((bf16[1,1,1,32,520]{4,3,2,1,0:T(8,128)(2,1)}, bf16[1,1,1,32,520]{4,3,2,1,0:T(8,128)(2,1)S(1)}, u32[]{:S(2)}, u32[]{:S(2)}) %collective-permute-start.2) | collective-permute-done | bytes 33312 | tf_op jit(solution)/shard_map/ppermute | solution.py:88
  57.3 0.6 copy-done.3
  57.9 2.1 %collective-permute-done.3 = bf16[1,1,1,32,520]{4,3,2,1,0:T(8,128)(2,1)} collective-permute-done((bf16[1,1,1,32,520]{4,3,2,1,0:T(8,128)(2,1)S(1)}, bf16[1,1,1,32,520]{4,3,2,1,0:T(8,128)(2,1)}, u32[]{:S(2)}, u32[]{:S(2)}) %collective-permute-start.3) | collective-permute-done | bytes 33312 | tf_op jit(solution)/shard_map/ppermute | solution.py:88
  60.0 0.8 fusion.78
  60.8 0.8 broadcast_multiply_fusion.3
  61.6 0.8 subtract_exponential_fusion.1
  62.6 1.6 %multiply_reduce_fusion.2 = (f32[32,4]{1,0:T(8,128)S(1)}, f32[32,4,64]{2,1,0:T(4,128)}, f32[32,4,64]{2,1,0:T(4,128)S(1)}, f32[32,4,64]{2,1,0:T(4,128)S(1)}) fusion(f32[32,4,64]{2,1,0:T(4,128)S(1)} %reshape.188, f32[32,4,64]{2,1,0:T(4,128)S(1)} %reshape.187, f32[32,4]{1,0:T(8,128)S(1)} %get-tuple-element.22, f32[32,4,64]{2,1,0:T(4,128)} %param.34, ...), kind=kLoop, calls=%fused_computation.67 | loop fusion | flops 57216 | bytes 231424 | tf_op jit(solution)/shard_map/reduce_sum | solution.py:43
  64.3 6.3 %multiply_reduce_fusion = (f32[32,4,64]{2,1,0:T(4,128)S(1)}, f32[32,4,64,64]{3,2,1,0:T(8,128)}) fusion(f32[32,4,64]{2,1,0:T(4,128)S(1)} %reshape.188, f32[32,4,64]{2,1,0:T(4,128)S(1)} %get-tuple-element.35, f32[32,4,64]{2,1,0:T(4,128)S(1)} %get-tuple-element.38, f32[32,4,64,64]{3,2,1,0:T(8,128)} %param.33, f32[32,4]{1,0:T(8,128)S(1)} %subtract_exponential_fusion.1), kind=kLoop, calls=%fused_computation | loop fusion | flops 2613248 | bytes 4325888 | tf_op jit(solution)/shard_map/reduce_sum | solution.py:42
  70.6 0.2 fusion.76
  70.8 0.2 multiply_reduce_fusion.1
  71.0 0.1 subtract_multiply_fusion
  71.3 1.6 %convolution_convert_fusion.1 = bf16[32,2048]{1,0:T(8,128)(2,1)S(1)} fusion(bf16[256,2048]{1,0:T(8,128)(2,1)} %all-gather.2.cloned.1.call-done, f32[32,256]{1,0:T(8,128)S(1)} %mul.194, bf16[32,520]{1,0:T(8,128)(2,1)S(1)} %get-tuple-element.27, f32[256]{0:T(256)S(1)} %copy-done.8), kind=kOutput, calls=%fused_computation.13 | convolution fusion | flops 33677312 | bytes 1229824 | tf_op jit(solution)/shard_map/dot_general | solution.py:188
  73.1 1.2 collective-permute-done.10
  74.3 0.2 fusion.33
  74.5 0.4 fusion.12
  74.9 19.9 %all_to_all.29 = bf16[16,8,2048]{2,1,0:T(8,128)(2,1)S(1)} all-to-all(bf16[16,8,2048]{2,1,0:T(8,128)(2,1)S(1)} %fusion.12), channel_id=1, replica_groups=mesh['ep'=16,'tp'=2] {'ep'}, dimensions={0} | all-to-all | bytes 1048576 | tf_op jit(solution)/shard_map/all_to_all | solution.py:198
  94.8 1.9 %collective-permute-done.11 = bf16[16,8,2048]{2,1,0:T(8,128)(2,1)S(1)} collective-permute-done((bf16[16,8,2048]{2,1,0:T(8,128)(2,1)S(1)}, bf16[16,8,2048]{2,1,0:T(8,128)(2,1)S(1)}, u32[]{:S(2)}, u32[]{:S(2)}) %collective-permute-start.11) | collective-permute-done | bytes 524320 | tf_op jit(solution)/shard_map/ppermute | solution.py:103
  96.7 0.8 copy-done.10
  97.5 1.8 %fusion.4 = f32[256,704]{0,1:T(8,128)} fusion(bf16[1,2048,704]{1,2,0:T(8,128)(2,1)S(1)} %copy-done.9, bf16[1,128,2048]{2,1,0:T(8,128)(2,1)S(1)} %bitcast.64, bf16[1,128,2048]{2,1,0:T(8,128)(2,1)S(1)} %bitcast.62), kind=kOutput, calls=%fused_computation.6 | convolution fusion | flops 740294656 | bytes 4653056 | tf_op jit(solution)/shard_map/xcd,xdf->xcf/dot_general | solution.py:206
  99.4 6.4 %fusion.9 = bf16[1,256,2048]{2,1,0:T(8,128)(2,1)} fusion(bf16[1,704,2048]{2,1,0:T(8,128)(2,1)S(1)} %copy-done, bf16[1,2048,704]{1,2,0:T(8,128)(2,1)} %param.38, f32[256,704]{0,1:T(8,128)} %fusion.4, bf16[1,128,2048]{2,1,0:T(8,128)(2,1)} %bitcast.65, bf16[1,128,2048]{2,1,0:T(8,128)(2,1)S(1)} %bitcast.63), kind=kOutput, calls=%fused_computation.9 | convolution fusion | flops 1480097792 | bytes 8585216 | tf_op jit(solution)/shard_map/xcf,xfd->xcd/dot_general | solution.py:211
  105.8 1.1 slice.43
  106.9 0.2 collective-permute-start.12
  107.0 1.8 %collective-permute-done.12 = bf16[1,128,2048]{2,1,0:T(8,128)(2,1)S(1)} collective-permute-done((bf16[1,128,2048]{2,1,0:T(8,128)(2,1)S(1)}, bf16[1,128,2048]{2,1,0:T(8,128)(2,1)S(1)}, u32[]{:S(2)}, u32[]{:S(2)}) %collective-permute-start.12) | collective-permute-done | bytes 524320 | tf_op jit(solution)/shard_map/ppermute | solution.py:103
  108.8 2.0 %fusion.24 = bf16[16,8,2048]{2,1,0:T(8,128)(2,1)} fusion(bf16[1,128,2048]{2,1,0:T(8,128)(2,1)S(1)} %collective-permute-done.12, bf16[1,256,2048]{2,1,0:T(8,128)(2,1)} %fusion.9), kind=kLoop, calls=%fused_computation.24 | loop fusion | flops 1048576 | bytes 1572864 | tf_op jit(solution)/shard_map/reshape;transpose;reshape | solution.py:221
  110.8 3.9 %all-to-all-start.2 = ((bf16[16,8,2048]{2,1,0:T(8,128)(2,1)}), bf16[16,8,2048]{2,1,0:T(8,128)(2,1)S(1)}, u32[]{:S(2)}, u32[]{:S(2)}) async-start(bf16[16,8,2048]{2,1,0:T(8,128)(2,1)} %fusion.24), calls=%async_computation.2 | async-start | bytes 1048576 | tf_op jit(solution)/shard_map/all_to_all | solution.py:222
  114.8 1.4 select_reduce_fusion
  116.2 14.0 %all-to-all-done.2 = bf16[16,8,2048]{2,1,0:T(8,128)(2,1)S(1)} async-done(((bf16[16,8,2048]{2,1,0:T(8,128)(2,1)}), bf16[16,8,2048]{2,1,0:T(8,128)(2,1)S(1)}, u32[]{:S(2)}, u32[]{:S(2)}) %all-to-all-start.2) | async-done | bytes 524320 | tf_op jit(solution)/shard_map/all_to_all | solution.py:222
  130.2 0.9 fusion.26
  131.1 1.7 %convolution_add_fusion = f32[32,2048]{1,0:T(8,128)} fusion(f32[32,2048]{1,0:T(8,128)S(1)} %fusion.26, bf16[16,8,2048]{2,1,0:T(8,128)(2,1)S(1)} %all-to-all-done.2, f32[32,128]{1,0:T(8,128)} %select_reduce_fusion), kind=kOutput, calls=%fused_computation.12 | convolution fusion | flops 16859136 | bytes 1064960 | tf_op jit(solution)/shard_map/dot_general | solution.py:227
  132.8 0.7 copy.67
  133.4 1.1 collective-permute-done.13
  134.5 1.6 %fusion.36 = bf16[32,2048]{1,0:T(8,128)(2,1)} fusion(bf16[32,2048]{1,0:T(8,128)(2,1)S(1)} %get-tuple-element.17, f32[32,2048]{1,0:T(8,128)} %convolution_add_fusion, f32[32,2048]{1,0:T(8,128)S(1)} %collective-permute-done.13), kind=kLoop, calls=%fused_computation.45 | loop fusion | flops 262144 | bytes 786432 | tf_op jit(solution)/shard_map/convert_element_type | solution.py:231
  (53 shorter events, 1.2 us)
Async XLA Ops:
  7.2 92.2 %copy-start = (bf16[1,704,2048]{2,1,0:T(8,128)(2,1)S(1)}, bf16[1,704,2048]{2,1,0:T(8,128)(2,1)}, u32[]{:S(2)}) copy-start(bf16[1,704,2048]{2,1,0:T(8,128)(2,1)} %param.39) | copy-start | bytes 8650756
  7.2 64.1 %all-gather.2.cloned.1.call-start = ((), (), s32[]{:S(2)}) async-start(), calls=%async_computation.3 | async-start | bytes 1114112 | tf_op jit(solution)/shard_map/all_gather | solution.py:132
  10.8 16.1 %all-to-all-start = ((bf16[32,16,128]{2,0,1:T(8,128)(2,1)}), bf16[32,16,128]{2,0,1:T(8,128)(2,1)S(1)}, u32[]{:S(2)}, u32[]{:S(2)}) async-start(bf16[32,16,128]{2,0,1:T(8,128)(2,1)} %copy_bitcast_fusion), calls=%async_computation | async-start | bytes 262144 | tf_op jit(solution)/shard_map/all_to_all | solution.py:151
  28.1 1.9 %copy-start.1 = (bf16[512,512]{1,0:T(8,128)(2,1)}, bf16[512,512]{1,0:T(8,128)(2,1)S(1)}, u32[]{:S(2)}) copy-start(bf16[512,512]{1,0:T(8,128)(2,1)S(1)} %convolution_convert_fusion.3) | copy-start | bytes 1572868
  28.9 6.9 %collective-permute-start.5 = (bf16[4,2,1,32,512]{4,3,2,1,0:T(8,128)(2,1)}, bf16[4,2,1,32,512]{4,3,2,1,0:T(8,128)(2,1)}, u32[]{:S(2)}, u32[]{:S(2)}) collective-permute-start(bf16[4,2,1,32,512]{4,3,2,1,0:T(8,128)(2,1)} %constant_dynamic-slice_fusion), channel_id=1, source_target_pairs={{0,2},{2,0},{4,6},{6,4},{8,10},{10,8},{12,14},{14,12},{16,18},{18,... | collective-permute-start | bytes 786440 | tf_op jit(solution)/shard_map/ppermute | solution.py:88
  33.4 10.9 %collective-permute-start = (bf16[4,1,2,32,520]{4,3,2,1,0:T(8,128)(2,1)S(1)}, bf16[4,1,2,32,520]{4,3,2,1,0:T(8,128)(2,1)S(1)}, u32[]{:S(2)}, u32[]{:S(2)}) collective-permute-start(bf16[4,1,2,32,520]{4,3,2,1,0:T(8,128)(2,1)S(1)} %constant_dynamic-slice_fusion.1), channel_id=1, source_target_pairs={{0,4},{2,6},{4,0},{6,2},{8,12},{10,14},{12,8},{14,10},{16,20},{18,... | collective-permute-start | bytes 798728 | tf_op jit(solution)/shard_map/ppermute | solution.py:88
  36.9 8.7 %collective-permute-start.6 = (bf16[4,1,1,32,512]{4,3,2,1,0:T(8,128)(2,1)S(1)}, bf16[4,1,1,32,512]{4,3,2,1,0:T(8,128)(2,1)S(1)}, u32[]{:S(2)}, u32[]{:S(2)}) collective-permute-start(bf16[4,1,1,32,512]{4,3,2,1,0:T(8,128)(2,1)S(1)} %dynamic-slice_convert_fusion.1), channel_id=1, source_target_pairs={{0,4},{2,6},{4,0},{6,2},{8,12},{10,14},{12,8},{14,10},{16,20},{18,... | collective-permute-start | bytes 393224 | tf_op jit(solution)/shard_map/ppermute | solution.py:88
  44.4 5.4 %collective-permute-start.1 = (bf16[4,1,1,32,520]{4,3,2,1,0:T(8,128)(2,1)S(1)}, bf16[4,1,1,32,520]{4,3,2,1,0:T(8,128)(2,1)S(1)}, u32[]{:S(2)}, u32[]{:S(2)}) collective-permute-start(bf16[4,1,1,32,520]{4,3,2,1,0:T(8,128)(2,1)S(1)} %dynamic-slice_convert_fusion), channel_id=1, source_target_pairs={{0,2},{2,0},{4,6},{6,4},{8,10},{10,8},{12,14},{14,12},{16,18},{18,... | collective-permute-start | bytes 399368 | tf_op jit(solution)/shard_map/ppermute | solution.py:88
  45.8 8.6 %collective-permute-start.7 = (bf16[1,1,1,32,512]{4,3,2,1,0:T(8,128)(2,1)S(1)}, bf16[1,1,1,32,512]{4,3,2,1,0:T(8,128)(2,1)S(1)}, u32[]{:S(2)}, u32[]{:S(2)}) collective-permute-start(bf16[1,1,1,32,512]{4,3,2,1,0:T(8,128)(2,1)S(1)} %get-tuple-element.32), channel_id=1, source_target_pairs={{0,8},{2,10},{4,12},{6,14},{8,16},{10,18},{12,20},{14,22},{16,24},... | collective-permute-start | bytes 98312 | tf_op jit(solution)/shard_map/ppermute | solution.py:88
  46.1 9.1 %collective-permute-start.9 = (bf16[1,1,1,32,512]{4,3,2,1,0:T(8,128)(2,1)S(1)}, bf16[1,1,1,32,512]{4,3,2,1,0:T(8,128)(2,1)S(1)}, u32[]{:S(2)}, u32[]{:S(2)}) collective-permute-start(bf16[1,1,1,32,512]{4,3,2,1,0:T(8,128)(2,1)S(1)} %get-tuple-element.33), channel_id=1, source_target_pairs={{0,24},{2,26},{4,28},{6,30},{8,0},{10,2},{12,4},{14,6},{16,8},{18,... | collective-permute-start | bytes 98312 | tf_op jit(solution)/shard_map/ppermute | solution.py:88
  49.6 5.7 %collective-permute-start.8 = (bf16[1,1,1,32,512]{4,3,2,1,0:T(8,128)(2,1)S(1)}, bf16[1,1,1,32,512]{4,3,2,1,0:T(8,128)(2,1)S(1)}, u32[]{:S(2)}, u32[]{:S(2)}) collective-permute-start(bf16[1,1,1,32,512]{4,3,2,1,0:T(8,128)(2,1)S(1)} %get-tuple-element.34), channel_id=1, source_target_pairs={{0,16},{2,18},{4,20},{6,22},{8,24},{10,26},{12,28},{14,30},{16,0},... | collective-permute-start | bytes 98312 | tf_op jit(solution)/shard_map/ppermute | solution.py:88
  50.5 6.8 %collective-permute-start.2 = (bf16[1,1,1,32,520]{4,3,2,1,0:T(8,128)(2,1)}, bf16[1,1,1,32,520]{4,3,2,1,0:T(8,128)(2,1)S(1)}, u32[]{:S(2)}, u32[]{:S(2)}) collective-permute-start(bf16[1,1,1,32,520]{4,3,2,1,0:T(8,128)(2,1)} %get-tuple-element.29), channel_id=1, source_target_pairs={{0,8},{2,10},{4,12},{6,14},{8,16},{10,18},{12,20},{14,22},{16,24},... | collective-permute-start | bytes 99848 | tf_op jit(solution)/shard_map/ppermute | solution.py:88
  51.0 6.3 %collective-permute-start.4 = (bf16[1,1,1,32,520]{4,3,2,1,0:T(8,128)(2,1)}, bf16[1,1,1,32,520]{4,3,2,1,0:T(8,128)(2,1)S(1)}, u32[]{:S(2)}, u32[]{:S(2)}) collective-permute-start(bf16[1,1,1,32,520]{4,3,2,1,0:T(8,128)(2,1)} %get-tuple-element.30), channel_id=1, source_target_pairs={{0,24},{2,26},{4,28},{6,30},{8,0},{10,2},{12,4},{14,6},{16,8},{18,... | collective-permute-start | bytes 99848 | tf_op jit(solution)/shard_map/ppermute | solution.py:88
  54.3 5.7 %collective-permute-start.3 = (bf16[1,1,1,32,520]{4,3,2,1,0:T(8,128)(2,1)S(1)}, bf16[1,1,1,32,520]{4,3,2,1,0:T(8,128)(2,1)}, u32[]{:S(2)}, u32[]{:S(2)}) collective-permute-start(bf16[1,1,1,32,520]{4,3,2,1,0:T(8,128)(2,1)S(1)} %get-tuple-element.31), channel_id=1, source_target_pairs={{0,16},{2,18},{4,20},{6,22},{8,24},{10,26},{12,28},{14,30},{16,0},... | collective-permute-start | bytes 99848 | tf_op jit(solution)/shard_map/ppermute | solution.py:88
  57.3 0.6 copy-start.3
  64.2 7.1 %copy-start.8 = (f32[256]{0:T(256)S(1)}, f32[256]{0:T(256)}, u32[]{:S(2)}) copy-start(f32[256]{0:T(256)} %param.31) | copy-start | bytes 3076
  64.2 8.8 %copy-start.6 = (s32[32,3]{0,1:T(4,128)S(1)}, s32[32,3]{0,1:T(4,128)}, u32[]{:S(2)}) copy-start(s32[32,3]{0,1:T(4,128)} %param.40) | copy-start | bytes 1156
  64.2 8.7 %copy-start.7 = (s32[32,3]{0,1:T(4,128)S(1)}, s32[32,3]{0,1:T(4,128)}, u32[]{:S(2)}) copy-start(s32[32,3]{0,1:T(4,128)} %copy.63) | copy-start | bytes 1156
  64.3 10.1 %copy-start.2 = (bf16[32,2048]{1,0:T(8,128)(2,1)S(1)}, bf16[32,2048]{1,0:T(8,128)(2,1)}, u32[]{:S(2)}) copy-start(bf16[32,2048]{1,0:T(8,128)(2,1)} %param.21) | copy-start | bytes 393220
  64.3 10.2 %copy-start.5 = (f32[2048]{0:T(1024)S(1)}, f32[2048]{0:T(1024)}, u32[]{:S(2)}) copy-start(f32[2048]{0:T(1024)} %param.36) | copy-start | bytes 24580
  71.3 26.3 %copy-start.9 = (bf16[1,2048,704]{1,2,0:T(8,128)(2,1)S(1)}, bf16[1,2048,704]{1,2,0:T(8,128)(2,1)}, u32[]{:S(2)}) copy-start(bf16[1,2048,704]{1,2,0:T(8,128)(2,1)} %param.37) | copy-start | bytes 8650756
  72.9 1.4 collective-permute-start.10
  73.0 1.5 %copy-start.4 = (s32[32,3]{0,1:T(4,128)}, s32[32,3]{0,1:T(4,128)S(1)}, u32[]{:S(2)}) copy-start(s32[32,3]{0,1:T(4,128)S(1)} %fusion.65) | copy-start | bytes 1156
  94.8 1.9 %collective-permute-start.11 = (bf16[16,8,2048]{2,1,0:T(8,128)(2,1)S(1)}, bf16[16,8,2048]{2,1,0:T(8,128)(2,1)S(1)}, u32[]{:S(2)}, u32[]{:S(2)}) collective-permute-start(bf16[16,8,2048]{2,1,0:T(8,128)(2,1)S(1)} %all_to_all.29), channel_id=1, source_target_pairs={{0,1},{1,0},{2,3},{3,2},{4,5},{5,4},{6,7},{7,6},{8,9},{9,8},{10,11... | collective-permute-start | bytes 1572872 | tf_op jit(solution)/shard_map/ppermute | solution.py:103
  96.7 0.8 copy-start.10
  106.9 2.0 %collective-permute-start.12 = (bf16[1,128,2048]{2,1,0:T(8,128)(2,1)S(1)}, bf16[1,128,2048]{2,1,0:T(8,128)(2,1)S(1)}, u32[]{:S(2)}, u32[]{:S(2)}) collective-permute-start(bf16[1,128,2048]{2,1,0:T(8,128)(2,1)S(1)} %slice.43), channel_id=1, source_target_pairs={{0,1},{1,0},{2,3},{3,2},{4,5},{5,4},{6,7},{7,6},{8,9},{9,8},{10,11... | collective-permute-start | bytes 1572872 | tf_op jit(solution)/shard_map/ppermute | solution.py:103
  110.8 19.3 %all-to-all-start.2 = ((bf16[16,8,2048]{2,1,0:T(8,128)(2,1)}), bf16[16,8,2048]{2,1,0:T(8,128)(2,1)S(1)}, u32[]{:S(2)}, u32[]{:S(2)}) async-start(bf16[16,8,2048]{2,1,0:T(8,128)(2,1)} %fusion.24), calls=%async_computation.2 | async-start | bytes 1048576 | tf_op jit(solution)/shard_map/all_to_all | solution.py:222
  132.8 1.7 %collective-permute-start.13 = (f32[32,2048]{1,0:T(8,128)}, f32[32,2048]{1,0:T(8,128)S(1)}, u32[]{:S(2)}, u32[]{:S(2)}) collective-permute-start(f32[32,2048]{1,0:T(8,128)} %convolution_add_fusion), channel_id=1, source_target_pairs={{0,1},{1,0},{2,3},{3,2},{4,5},{5,4},{6,7},{7,6},{8,9},{9,8},{10,11... | collective-permute-start | bytes 786440 | tf_op jit(solution)/shard_map/ppermute | solution.py:103
Sparse Core Ops, SparseCore 0:
  10.7 57.9 all-gather.1
where the time goes:
time: 144 us; the launch traced here: 143 us
  waiting for transfers between devices  36.3 us (25%)
  starting transfers between devices  24.3 us (17%)
  other arithmetic  20.7 us (14%)
  blocking collectives  19.9 us (14%)
  matrix products  16 us (11%)
  between operations  14.5 us (10%)
  local copies, waits for them, and re-layouts  11.1 us (8%)
    all_to_all x1, blocking collectives, body(): lax.all_to_all(outgoing, 'ep', split_axis=0, concat_axis=0, tiled=True)  19.9 us
    all_to_all x1, waiting for transfers between devices, body(): lax.all_to_all(finished, 'ep', split_axis=0, concat_axis=0, tiled=True)  14 us
    ppermute x10, waiting for transfers between devices, reduce_stage(): lax.ppermute(sent.astype(jnp.bfloat16), 'ep', shift_pairs(factors, axis,...  13.1 us
    ppermute x10, starting transfers between devices, reduce_stage(): lax.ppermute(sent.astype(jnp.bfloat16), 'ep', shift_pairs(factors, axis,...  11.8 us
    all_to_all x1, starting transfers between devices, body(): lax.all_to_all(normed, 'ep', split_axis=1, concat_axis=0, tiled=True)  8.34 us
    dot_general x1, matrix products, body(): jnp.einsum('xcf,xfd->xcd', hidden, w_expert_down, preferred_element_type=...  6.4 us
    reduce_sum x1, other arithmetic, memory_cell(): numerator = jnp.sum(new_matrix * query_heads[:, :, None, :], axis=-1)  6.35 us
    ppermute x4, waiting for transfers between devices, swap_cores(): return lax.ppermute(values_in, 'tp', [(0, 1), (1, 0)])  5.98 us
  transfers between devices with their start and end apart: 17, of which 12 were waited for; matrix products, arithmetic and copies ran while one was open for 20% of the time, Pallas kernels for 0%

commit v1 on v0

--- a/solution.py
+++ b/solution.py
@@ -148,7 +148,10 @@
     token_hits = jnp.any(hits, axis=1).astype(jnp.bfloat16)
     weight_hits = jnp.sum(jnp.where(hits, route_weights[:, :, None], 0.0), axis=1)
     normed = rms_scale(tokens, mix_gain).astype(jnp.bfloat16)
-    spread = lax.all_to_all(normed, "ep", split_axis=1, concat_axis=0, tiled=True)
+    spread = jnp.concatenate(
+        lax.all_to_all(jnp.stack(jnp.split(normed, lax.axis_size("ep"), axis=1)), "ep", 0, 0),
+        axis=0,
+    )
     first_list = (w_query, w_key)
     second_list = (w_value, w_outgate, w_igate, w_fgate)
     first = staged_reduce_scatter(

time: 144 us -> 153 us (1.062)
  local copies, waits for them, and re-layouts: 11.1 us -> 20.8 us
  waiting for transfers between devices: 36.3 us -> 38.3 us
    unnamed x27 -> x46, local copies, waits for them, and re-layouts: 5.88 us -> 14.9 us
    ppermute x10, waiting for transfers between devices: 13.1 us -> 15.1 us  [reduce_stage(): lax.ppermute(sent.astype(jnp.bfloat16), 'ep', shift_pairs(factors, axis,...]
    all_to_all x1 -> x0, other arithmetic: 1.67 us -> none  [body(): lax.all_to_all(normed, 'ep', split_axis=1, concat_axis=0, tiled=True)]
  transfers between devices with their start and end apart: 17 -> 17, of which waited for: 12 -> 12; matrix products, arithmetic and copies ran while one was open for 20% -> 24% of each run, Pallas kernels for 0% -> 0%
where the time goes in v1:
time: 153 us; the launch traced here: 151 us
  waiting for transfers between devices  38.3 us (25%)
  starting transfers between devices  23.4 us (15%)
  local copies, waits for them, and re-layouts  20.8 us (14%)
  other arithmetic  20.1 us (13%)
  blocking collectives  19.2 us (13%)
  matrix products  15.2 us (10%)
  between operations  14.6 us (10%)
    all_to_all x1, blocking collectives, body(): lax.all_to_all(outgoing, 'ep', split_axis=0, concat_axis=0, tiled=True)  19.2 us
    ppermute x10, waiting for transfers between devices, reduce_stage(): lax.ppermute(sent.astype(jnp.bfloat16), 'ep', shift_pairs(factors, axis,...  15.1 us
    unnamed x46, local copies, waits for them, and re-layouts  14.9 us
    all_to_all x1, waiting for transfers between devices, body(): lax.all_to_all(finished, 'ep', split_axis=0, concat_axis=0, tiled=True)  14 us
    ppermute x10, starting transfers between devices, reduce_stage(): lax.ppermute(sent.astype(jnp.bfloat16), 'ep', shift_pairs(factors, axis,...  10.8 us
    all_to_all x1, starting transfers between devices, body(): lax.all_to_all(jnp.stack(jnp.split(normed, lax.axis_size('ep'), axis=1)),...  8.34 us
    dot_general x1, matrix products, body(): jnp.einsum('xcf,xfd->xcd', hidden, w_expert_down, preferred_element_type=...  6.4 us
    reduce_sum x1, other arithmetic, memory_cell(): numerator = jnp.sum(new_matrix * query_heads[:, :, None, :], axis=-1)  6.34 us
  transfers between devices with their start and end apart: 17, of which 12 were waited for; matrix products, arithmetic and copies ran while one was open for 24% of the time, Pallas kernels for 0%

profile of v1, /device:TPU:0, one launch (start us, length us, event | category | flops | bytes accessed | tf_op | source)
XLA Modules:
  0.0 151.5 jit_solution(15241356886433280603)
XLA Ops:
  7.2 0.7 all-gather.2.cloned.1.call-update
  7.9 1.2 fusion.29
  9.1 1.0 fusion.31
  10.1 0.6 constant_dynamic-update-slice_fusion.15
  10.7 0.6 constant_dynamic-update-slice_fusion.14
  11.3 0.6 constant_dynamic-update-slice_fusion.13
  11.9 0.6 constant_dynamic-update-slice_fusion.12
  12.5 0.6 constant_dynamic-update-slice_fusion.11
  13.1 0.6 constant_dynamic-update-slice_fusion.10
  14.3 0.6 constant_dynamic-update-slice_fusion.8
  14.9 0.6 constant_dynamic-update-slice_fusion.7
  15.5 0.6 constant_dynamic-update-slice_fusion.6
  16.1 0.6 constant_dynamic-update-slice_fusion.5
  16.7 0.6 constant_dynamic-update-slice_fusion.4
  17.4 0.6 constant_dynamic-update-slice_fusion.3
  18.0 0.6 constant_dynamic-update-slice_fusion.2
  18.6 0.6 constant_dynamic-update-slice_fusion.1
  19.8 8.3 %all-to-all-start = ((bf16[16,32,128]{2,1,0:T(8,128)(2,1)}), bf16[16,32,128]{2,1,0:T(8,128)(2,1)S(1)}, u32[]{:S(2)}, u32[]{:S(2)}) async-start(bf16[16,32,128]{2,1,0:T(8,128)(2,1)} %constant_dynamic-update-slice_fusion), calls=%async_computation | async-start | bytes 262144 | tf_op jit(solution)/shard_map/all_to_all | solution.py:152
  28.2 1.4 copy.58
  29.6 0.8 copy.59
  30.5 0.8 copy.55
  31.3 0.8 copy.56
  32.6 0.7 copy.60
  33.3 2.6 %all-to-all-done = bf16[16,32,128]{2,1,0:T(8,128)(2,1)S(1)} async-done(((bf16[16,32,128]{2,1,0:T(8,128)(2,1)}), bf16[16,32,128]{2,1,0:T(8,128)(2,1)S(1)}, u32[]{:S(2)}, u32[]{:S(2)}) %all-to-all-start) | async-done | bytes 131104 | tf_op jit(solution)/shard_map/all_to_all | solution.py:152
  35.9 1.2 convolution_convert_fusion.3
  37.1 0.8 constant_dynamic-slice_fusion
  37.9 1.1 collective-permute-start.5
  39.0 1.1 convolution_convert_fusion.2
  40.1 1.3 copy.57
  41.8 3.0 %collective-permute-done.5 = bf16[4,2,1,32,512]{4,3,2,1,0:T(8,128)(2,1)} collective-permute-done((bf16[4,2,1,32,512]{4,3,2,1,0:T(8,128)(2,1)}, bf16[4,2,1,32,512]{4,3,2,1,0:T(8,128)(2,1)}, u32[]{:S(2)}, u32[]{:S(2)}) %collective-permute-start.5) | collective-permute-done | bytes 262176 | tf_op jit(solution)/shard_map/ppermute | solution.py:88
  44.8 1.1 convert_add_fusion.1
  46.0 1.0 collective-permute-start.6
  47.0 4.0 %collective-permute-done = bf16[4,1,2,32,520]{4,3,2,1,0:T(8,128)(2,1)S(1)} collective-permute-done((bf16[4,1,2,32,520]{4,3,2,1,0:T(8,128)(2,1)S(1)}, bf16[4,1,2,32,520]{4,3,2,1,0:T(8,128)(2,1)S(1)}, u32[]{:S(2)}, u32[]{:S(2)}) %collective-permute-start) | collective-permute-done | bytes 266272 | tf_op jit(solution)/shard_map/ppermute | solution.py:88
  51.1 0.7 collective-permute-start.1
  52.8 3.6 %collective-permute-start.9 = (bf16[1,1,1,32,512]{4,3,2,1,0:T(8,128)(2,1)S(1)}, bf16[1,1,1,32,512]{4,3,2,1,0:T(8,128)(2,1)S(1)}, u32[]{:S(2)}, u32[]{:S(2)}) collective-permute-start(bf16[1,1,1,32,512]{4,3,2,1,0:T(8,128)(2,1)S(1)} %get-tuple-element.33), channel_id=1, source_target_pairs={{0,24},{2,26},{4,28},{6,30},{8,0},{10,2},{12,4},{14,6},{16,8},{18,... | collective-permute-start | bytes 98312 | tf_op jit(solution)/shard_map/ppermute | solution.py:88
  56.4 3.3 %collective-permute-done.1 = bf16[4,1,1,32,520]{4,3,2,1,0:T(8,128)(2,1)S(1)} collective-permute-done((bf16[4,1,1,32,520]{4,3,2,1,0:T(8,128)(2,1)S(1)}, bf16[4,1,1,32,520]{4,3,2,1,0:T(8,128)(2,1)S(1)}, u32[]{:S(2)}, u32[]{:S(2)}) %collective-permute-start.1) | collective-permute-done | bytes 133152 | tf_op jit(solution)/shard_map/ppermute | solution.py:88
  59.7 0.7 dynamic-slice_convert_fusion.4
  60.8 3.4 %collective-permute-start.4 = (bf16[1,1,1,32,520]{4,3,2,1,0:T(8,128)(2,1)}, bf16[1,1,1,32,520]{4,3,2,1,0:T(8,128)(2,1)S(1)}, u32[]{:S(2)}, u32[]{:S(2)}) collective-permute-start(bf16[1,1,1,32,520]{4,3,2,1,0:T(8,128)(2,1)} %get-tuple-element.30), channel_id=1, source_target_pairs={{0,24},{2,26},{4,28},{6,30},{8,0},{10,2},{12,4},{14,6},{16,8},{18,... | collective-permute-start | bytes 99848 | tf_op jit(solution)/shard_map/ppermute | solution.py:88
  64.4 1.9 %collective-permute-done.2 = bf16[1,1,1,32,520]{4,3,2,1,0:T(8,128)(2,1)S(1)} collective-permute-done((bf16[1,1,1,32,520]{4,3,2,1,0:T(8,128)(2,1)}, bf16[1,1,1,32,520]{4,3,2,1,0:T(8,128)(2,1)S(1)}, u32[]{:S(2)}, u32[]{:S(2)}) %collective-permute-start.2) | collective-permute-done | bytes 33312 | tf_op jit(solution)/shard_map/ppermute | solution.py:88
  66.4 0.6 copy-done.5
  67.0 2.2 %collective-permute-done.3 = bf16[1,1,1,32,520]{4,3,2,1,0:T(8,128)(2,1)} collective-permute-done((bf16[1,1,1,32,520]{4,3,2,1,0:T(8,128)(2,1)S(1)}, bf16[1,1,1,32,520]{4,3,2,1,0:T(8,128)(2,1)}, u32[]{:S(2)}, u32[]{:S(2)}) %collective-permute-start.3) | collective-permute-done | bytes 33312 | tf_op jit(solution)/shard_map/ppermute | solution.py:88
  69.2 0.8 fusion.77
  70.0 0.8 broadcast_multiply_fusion.3
  70.8 0.8 subtract_exponential_fusion.1
  71.8 1.6 %multiply_reduce_fusion.2 = (f32[32,4]{1,0:T(8,128)S(1)}, f32[32,4,64]{2,1,0:T(4,128)}, f32[32,4,64]{2,1,0:T(4,128)S(1)}, f32[32,4,64]{2,1,0:T(4,128)S(1)}) fusion(f32[32,4,64]{2,1,0:T(4,128)S(1)} %reshape.189, f32[32,4,64]{2,1,0:T(4,128)S(1)} %reshape.188, f32[32,4]{1,0:T(8,128)S(1)} %get-tuple-element.22, f32[32,4,64]{2,1,0:T(4,128)} %param.34, ...), kind=kLoop, calls=%fused_computation.65 | loop fusion | flops 57216 | bytes 231424 | tf_op jit(solution)/shard_map/reduce_sum | solution.py:43
  73.5 6.3 %multiply_reduce_fusion = (f32[32,4,64]{2,1,0:T(4,128)S(1)}, f32[32,4,64,64]{3,2,1,0:T(8,128)}) fusion(f32[32,4,64]{2,1,0:T(4,128)S(1)} %reshape.189, f32[32,4,64]{2,1,0:T(4,128)S(1)} %get-tuple-element.35, f32[32,4,64]{2,1,0:T(4,128)S(1)} %get-tuple-element.38, f32[32,4,64,64]{3,2,1,0:T(8,128)} %param.33, f32[32,4]{1,0:T(8,128)S(1)} %subtract_exponential_fusion.1), kind=kLoop, calls=%fused_computation | loop fusion | flops 2613248 | bytes 4325888 | tf_op jit(solution)/shard_map/reduce_sum | solution.py:42
  80.5 1.6 %convolution_convert_fusion.1 = bf16[32,2048]{1,0:T(8,128)(2,1)S(1)} fusion(bf16[256,2048]{1,0:T(8,128)(2,1)} %all-gather.2.cloned.1.call-done, f32[32,256]{1,0:T(8,128)S(1)} %mul.194, bf16[32,520]{1,0:T(8,128)(2,1)S(1)} %get-tuple-element.27, f32[256]{0:T(256)S(1)} %copy-done.10), kind=kOutput, calls=%fused_computation.13 | convolution fusion | flops 33677312 | bytes 1229824 | tf_op jit(solution)/shard_map/dot_general | solution.py:191
  82.3 1.2 collective-permute-done.10
  84.1 19.2 %all_to_all.15 = bf16[16,8,2048]{2,1,0:T(8,128)(2,1)S(1)} all-to-all(bf16[16,8,2048]{2,1,0:T(8,128)(2,1)S(1)} %fusion.12), channel_id=1, replica_groups=mesh['ep'=16,'tp'=2] {'ep'}, dimensions={0} | all-to-all | bytes 1048576 | tf_op jit(solution)/shard_map/all_to_all | solution.py:201
  103.2 1.9 %collective-permute-done.11 = bf16[16,8,2048]{2,1,0:T(8,128)(2,1)S(1)} collective-permute-done((bf16[16,8,2048]{2,1,0:T(8,128)(2,1)S(1)}, bf16[16,8,2048]{2,1,0:T(8,128)(2,1)S(1)}, u32[]{:S(2)}, u32[]{:S(2)}) %collective-permute-start.11) | collective-permute-done | bytes 524320 | tf_op jit(solution)/shard_map/ppermute | solution.py:103
  105.2 0.8 copy-done.12
  106.0 1.9 %fusion.4 = f32[256,704]{0,1:T(8,128)} fusion(bf16[1,2048,704]{1,2,0:T(8,128)(2,1)S(1)} %copy-done.11, bf16[1,128,2048]{2,1,0:T(8,128)(2,1)S(1)} %bitcast.121, bf16[1,128,2048]{2,1,0:T(8,128)(2,1)S(1)} %bitcast.119), kind=kOutput, calls=%fused_computation.6 | convolution fusion | flops 740294656 | bytes 4653056 | tf_op jit(solution)/shard_map/xcd,xdf->xcf/dot_general | solution.py:209
  107.8 6.4 %fusion.9 = bf16[1,256,2048]{2,1,0:T(8,128)(2,1)} fusion(bf16[1,704,2048]{2,1,0:T(8,128)(2,1)S(1)} %copy-done, bf16[1,2048,704]{1,2,0:T(8,128)(2,1)} %param.38, f32[256,704]{0,1:T(8,128)} %fusion.4, bf16[1,128,2048]{2,1,0:T(8,128)(2,1)} %bitcast.122, bf16[1,128,2048]{2,1,0:T(8,128)(2,1)S(1)} %bitcast.120), kind=kOutput, calls=%fused_computation.9 | convolution fusion | flops 1480097792 | bytes 8585216 | tf_op jit(solution)/shard_map/xcf,xfd->xcd/dot_general | solution.py:214
  114.2 1.1 slice.43
  115.5 1.8 %collective-permute-done.12 = bf16[1,128,2048]{2,1,0:T(8,128)(2,1)S(1)} collective-permute-done((bf16[1,128,2048]{2,1,0:T(8,128)(2,1)S(1)}, bf16[1,128,2048]{2,1,0:T(8,128)(2,1)S(1)}, u32[]{:S(2)}, u32[]{:S(2)}) %collective-permute-start.12) | collective-permute-done | bytes 524320 | tf_op jit(solution)/shard_map/ppermute | solution.py:103
  117.3 2.0 %fusion.24 = bf16[16,8,2048]{2,1,0:T(8,128)(2,1)} fusion(bf16[1,128,2048]{2,1,0:T(8,128)(2,1)S(1)} %collective-permute-done.12, bf16[1,256,2048]{2,1,0:T(8,128)(2,1)} %fusion.9), kind=kLoop, calls=%fused_computation.24 | loop fusion | flops 1048576 | bytes 1572864 | tf_op jit(solution)/shard_map/reshape;transpose;reshape | solution.py:224
  119.3 3.9 %all-to-all-start.2 = ((bf16[16,8,2048]{2,1,0:T(8,128)(2,1)}), bf16[16,8,2048]{2,1,0:T(8,128)(2,1)S(1)}, u32[]{:S(2)}, u32[]{:S(2)}) async-start(bf16[16,8,2048]{2,1,0:T(8,128)(2,1)} %fusion.24), calls=%async_computation.2 | async-start | bytes 1048576 | tf_op jit(solution)/shard_map/all_to_all | solution.py:225
  123.2 1.4 select_reduce_fusion
  124.6 14.0 %all-to-all-done.2 = bf16[16,8,2048]{2,1,0:T(8,128)(2,1)S(1)} async-done(((bf16[16,8,2048]{2,1,0:T(8,128)(2,1)}), bf16[16,8,2048]{2,1,0:T(8,128)(2,1)S(1)}, u32[]{:S(2)}, u32[]{:S(2)}) %all-to-all-start.2) | async-done | bytes 524320 | tf_op jit(solution)/shard_map/all_to_all | solution.py:225
  138.6 0.9 fusion.26
  139.5 1.7 %convolution_add_fusion = f32[32,2048]{1,0:T(8,128)} fusion(f32[32,2048]{1,0:T(8,128)S(1)} %fusion.26, bf16[16,8,2048]{2,1,0:T(8,128)(2,1)S(1)} %all-to-all-done.2, f32[32,128]{1,0:T(8,128)} %select_reduce_fusion), kind=kOutput, calls=%fused_computation.12 | convolution fusion | flops 16859136 | bytes 1064960 | tf_op jit(solution)/shard_map/dot_general | solution.py:230
  141.2 0.7 copy.64
  141.9 1.1 collective-permute-done.13
  143.0 1.6 %fusion.36 = bf16[32,2048]{1,0:T(8,128)(2,1)} fusion(bf16[32,2048]{1,0:T(8,128)(2,1)S(1)} %get-tuple-element.17, f32[32,2048]{1,0:T(8,128)} %convolution_add_fusion, f32[32,2048]{1,0:T(8,128)S(1)} %collective-permute-done.13), kind=kLoop, calls=%fused_computation.45 | loop fusion | flops 262144 | bytes 786432 | tf_op jit(solution)/shard_map/convert_element_type | solution.py:234
  (73 shorter events, 5.6 us)
Async XLA Ops:
  7.2 100.7 %copy-start = (bf16[1,704,2048]{2,1,0:T(8,128)(2,1)S(1)}, bf16[1,704,2048]{2,1,0:T(8,128)(2,1)}, u32[]{:S(2)}) copy-start(bf16[1,704,2048]{2,1,0:T(8,128)(2,1)} %param.39) | copy-start | bytes 8650756
  7.2 31.8 %copy-start.3 = (bf16[128,256]{1,0:T(8,128)(2,1)S(1)}, bf16[128,256]{1,0:T(8,128)(2,1)}, u32[]{:S(2)}) copy-start(bf16[128,256]{1,0:T(8,128)(2,1)} %param.26) | copy-start | bytes 196612
  7.2 31.8 %copy-start.4 = (bf16[128,256]{1,0:T(8,128)(2,1)S(1)}, bf16[128,256]{1,0:T(8,128)(2,1)}, u32[]{:S(2)}) copy-start(bf16[128,256]{1,0:T(8,128)(2,1)} %param.25) | copy-start | bytes 196612
  7.2 73.3 %all-gather.2.cloned.1.call-start = ((), (), s32[]{:S(2)}) async-start(), calls=%async_computation.3 | async-start | bytes 1114112 | tf_op jit(solution)/shard_map/all_gather | solution.py:132
  19.8 16.1 %all-to-all-start = ((bf16[16,32,128]{2,1,0:T(8,128)(2,1)}), bf16[16,32,128]{2,1,0:T(8,128)(2,1)S(1)}, u32[]{:S(2)}, u32[]{:S(2)}) async-start(bf16[16,32,128]{2,1,0:T(8,128)(2,1)} %constant_dynamic-update-slice_fusion), calls=%async_computation | async-start | bytes 262144 | tf_op jit(solution)/shard_map/all_to_all | solution.py:152
  37.1 1.9 %copy-start.1 = (bf16[512,512]{1,0:T(8,128)(2,1)}, bf16[512,512]{1,0:T(8,128)(2,1)S(1)}, u32[]{:S(2)}) copy-start(bf16[512,512]{1,0:T(8,128)(2,1)S(1)} %convolution_convert_fusion.3) | copy-start | bytes 1572868
  37.9 6.9 %collective-permute-start.5 = (bf16[4,2,1,32,512]{4,3,2,1,0:T(8,128)(2,1)}, bf16[4,2,1,32,512]{4,3,2,1,0:T(8,128)(2,1)}, u32[]{:S(2)}, u32[]{:S(2)}) collective-permute-start(bf16[4,2,1,32,512]{4,3,2,1,0:T(8,128)(2,1)} %constant_dynamic-slice_fusion), channel_id=1, source_target_pairs={{0,2},{2,0},{4,6},{6,4},{8,10},{10,8},{12,14},{14,12},{16,18},{18,... | collective-permute-start | bytes 786440 | tf_op jit(solution)/shard_map/ppermute | solution.py:88
  41.5 9.5 %collective-permute-start = (bf16[4,1,2,32,520]{4,3,2,1,0:T(8,128)(2,1)S(1)}, bf16[4,1,2,32,520]{4,3,2,1,0:T(8,128)(2,1)S(1)}, u32[]{:S(2)}, u32[]{:S(2)}) collective-permute-start(bf16[4,1,2,32,520]{4,3,2,1,0:T(8,128)(2,1)S(1)} %constant_dynamic-slice_fusion.1), channel_id=1, source_target_pairs={{0,4},{2,6},{4,0},{6,2},{8,12},{10,14},{12,8},{14,10},{16,20},{18,... | collective-permute-start | bytes 798728 | tf_op jit(solution)/shard_map/ppermute | solution.py:88
  46.0 6.5 %collective-permute-start.6 = (bf16[4,1,1,32,512]{4,3,2,1,0:T(8,128)(2,1)S(1)}, bf16[4,1,1,32,512]{4,3,2,1,0:T(8,128)(2,1)S(1)}, u32[]{:S(2)}, u32[]{:S(2)}) collective-permute-start(bf16[4,1,1,32,512]{4,3,2,1,0:T(8,128)(2,1)S(1)} %dynamic-slice_convert_fusion.1), channel_id=1, source_target_pairs={{0,4},{2,6},{4,0},{6,2},{8,12},{10,14},{12,8},{14,10},{16,20},{18,... | collective-permute-start | bytes 393224 | tf_op jit(solution)/shard_map/ppermute | solution.py:88
  51.1 8.5 %collective-permute-start.1 = (bf16[4,1,1,32,520]{4,3,2,1,0:T(8,128)(2,1)S(1)}, bf16[4,1,1,32,520]{4,3,2,1,0:T(8,128)(2,1)S(1)}, u32[]{:S(2)}, u32[]{:S(2)}) collective-permute-start(bf16[4,1,1,32,520]{4,3,2,1,0:T(8,128)(2,1)S(1)} %dynamic-slice_convert_fusion), channel_id=1, source_target_pairs={{0,2},{2,0},{4,6},{6,4},{8,10},{10,8},{12,14},{14,12},{16,18},{18,... | collective-permute-start | bytes 399368 | tf_op jit(solution)/shard_map/ppermute | solution.py:88
  52.5 11.7 %collective-permute-start.7 = (bf16[1,1,1,32,512]{4,3,2,1,0:T(8,128)(2,1)S(1)}, bf16[1,1,1,32,512]{4,3,2,1,0:T(8,128)(2,1)S(1)}, u32[]{:S(2)}, u32[]{:S(2)}) collective-permute-start(bf16[1,1,1,32,512]{4,3,2,1,0:T(8,128)(2,1)S(1)} %get-tuple-element.32), channel_id=1, source_target_pairs={{0,8},{2,10},{4,12},{6,14},{8,16},{10,18},{12,20},{14,22},{16,24},... | collective-permute-start | bytes 98312 | tf_op jit(solution)/shard_map/ppermute | solution.py:88
  52.8 11.4 %collective-permute-start.9 = (bf16[1,1,1,32,512]{4,3,2,1,0:T(8,128)(2,1)S(1)}, bf16[1,1,1,32,512]{4,3,2,1,0:T(8,128)(2,1)S(1)}, u32[]{:S(2)}, u32[]{:S(2)}) collective-permute-start(bf16[1,1,1,32,512]{4,3,2,1,0:T(8,128)(2,1)S(1)} %get-tuple-element.33), channel_id=1, source_target_pairs={{0,24},{2,26},{4,28},{6,30},{8,0},{10,2},{12,4},{14,6},{16,8},{18,... | collective-permute-start | bytes 98312 | tf_op jit(solution)/shard_map/ppermute | solution.py:88
  56.4 7.8 %collective-permute-start.8 = (bf16[1,1,1,32,512]{4,3,2,1,0:T(8,128)(2,1)S(1)}, bf16[1,1,1,32,512]{4,3,2,1,0:T(8,128)(2,1)S(1)}, u32[]{:S(2)}, u32[]{:S(2)}) collective-permute-start(bf16[1,1,1,32,512]{4,3,2,1,0:T(8,128)(2,1)S(1)} %get-tuple-element.34), channel_id=1, source_target_pairs={{0,16},{2,18},{4,20},{6,22},{8,24},{10,26},{12,28},{14,30},{16,0},... | collective-permute-start | bytes 98312 | tf_op jit(solution)/shard_map/ppermute | solution.py:88
  60.3 6.0 %collective-permute-start.2 = (bf16[1,1,1,32,520]{4,3,2,1,0:T(8,128)(2,1)}, bf16[1,1,1,32,520]{4,3,2,1,0:T(8,128)(2,1)S(1)}, u32[]{:S(2)}, u32[]{:S(2)}) collective-permute-start(bf16[1,1,1,32,520]{4,3,2,1,0:T(8,128)(2,1)} %get-tuple-element.29), channel_id=1, source_target_pairs={{0,8},{2,10},{4,12},{6,14},{8,16},{10,18},{12,20},{14,22},{16,24},... | collective-permute-start | bytes 99848 | tf_op jit(solution)/shard_map/ppermute | solution.py:88
  60.8 5.6 %collective-permute-start.4 = (bf16[1,1,1,32,520]{4,3,2,1,0:T(8,128)(2,1)}, bf16[1,1,1,32,520]{4,3,2,1,0:T(8,128)(2,1)S(1)}, u32[]{:S(2)}, u32[]{:S(2)}) collective-permute-start(bf16[1,1,1,32,520]{4,3,2,1,0:T(8,128)(2,1)} %get-tuple-element.30), channel_id=1, source_target_pairs={{0,24},{2,26},{4,28},{6,30},{8,0},{10,2},{12,4},{14,6},{16,8},{18,... | collective-permute-start | bytes 99848 | tf_op jit(solution)/shard_map/ppermute | solution.py:88
  64.2 5.0 %collective-permute-start.3 = (bf16[1,1,1,32,520]{4,3,2,1,0:T(8,128)(2,1)S(1)}, bf16[1,1,1,32,520]{4,3,2,1,0:T(8,128)(2,1)}, u32[]{:S(2)}, u32[]{:S(2)}) collective-permute-start(bf16[1,1,1,32,520]{4,3,2,1,0:T(8,128)(2,1)S(1)} %get-tuple-element.31), channel_id=1, source_target_pairs={{0,16},{2,18},{4,20},{6,22},{8,24},{10,26},{12,28},{14,30},{16,0},... | collective-permute-start | bytes 99848 | tf_op jit(solution)/shard_map/ppermute | solution.py:88
  66.4 0.6 copy-start.5
  73.4 7.1 %copy-start.10 = (f32[256]{0:T(256)S(1)}, f32[256]{0:T(256)}, u32[]{:S(2)}) copy-start(f32[256]{0:T(256)} %param.31) | copy-start | bytes 3076
  73.4 8.8 %copy-start.8 = (s32[32,3]{0,1:T(4,128)S(1)}, s32[32,3]{0,1:T(4,128)}, u32[]{:S(2)}) copy-start(s32[32,3]{0,1:T(4,128)} %param.40) | copy-start | bytes 1156
  73.4 8.7 %copy-start.9 = (s32[32,3]{0,1:T(4,128)S(1)}, s32[32,3]{0,1:T(4,128)}, u32[]{:S(2)}) copy-start(s32[32,3]{0,1:T(4,128)} %copy.60) | copy-start | bytes 1156
  73.4 10.1 %copy-start.2 = (bf16[32,2048]{1,0:T(8,128)(2,1)S(1)}, bf16[32,2048]{1,0:T(8,128)(2,1)}, u32[]{:S(2)}) copy-start(bf16[32,2048]{1,0:T(8,128)(2,1)} %param.21) | copy-start | bytes 393220
  73.5 10.2 %copy-start.7 = (f32[2048]{0:T(1024)S(1)}, f32[2048]{0:T(1024)}, u32[]{:S(2)}) copy-start(f32[2048]{0:T(1024)} %param.36) | copy-start | bytes 24580
  80.5 25.5 %copy-start.11 = (bf16[1,2048,704]{1,2,0:T(8,128)(2,1)S(1)}, bf16[1,2048,704]{1,2,0:T(8,128)(2,1)}, u32[]{:S(2)}) copy-start(bf16[1,2048,704]{1,2,0:T(8,128)(2,1)} %param.37) | copy-start | bytes 8650756
  82.1 1.4 collective-permute-start.10
  82.2 1.5 copy-start.6
  103.2 1.9 %collective-permute-start.11 = (bf16[16,8,2048]{2,1,0:T(8,128)(2,1)S(1)}, bf16[16,8,2048]{2,1,0:T(8,128)(2,1)S(1)}, u32[]{:S(2)}, u32[]{:S(2)}) collective-permute-start(bf16[16,8,2048]{2,1,0:T(8,128)(2,1)S(1)} %all_to_all.15), channel_id=1, source_target_pairs={{0,1},{1,0},{2,3},{3,2},{4,5},{5,4},{6,7},{7,6},{8,9},{9,8},{10,11... | collective-permute-start | bytes 1572872 | tf_op jit(solution)/shard_map/ppermute | solution.py:103
  105.2 0.8 copy-start.12
  115.3 2.0 %collective-permute-start.12 = (bf16[1,128,2048]{2,1,0:T(8,128)(2,1)S(1)}, bf16[1,128,2048]{2,1,0:T(8,128)(2,1)S(1)}, u32[]{:S(2)}, u32[]{:S(2)}) collective-permute-start(bf16[1,128,2048]{2,1,0:T(8,128)(2,1)S(1)} %slice.43), channel_id=1, source_target_pairs={{0,1},{1,0},{2,3},{3,2},{4,5},{5,4},{6,7},{7,6},{8,9},{9,8},{10,11... | collective-permute-start | bytes 1572872 | tf_op jit(solution)/shard_map/ppermute | solution.py:103
  119.3 19.3 %all-to-all-start.2 = ((bf16[16,8,2048]{2,1,0:T(8,128)(2,1)}), bf16[16,8,2048]{2,1,0:T(8,128)(2,1)S(1)}, u32[]{:S(2)}, u32[]{:S(2)}) async-start(bf16[16,8,2048]{2,1,0:T(8,128)(2,1)} %fusion.24), calls=%async_computation.2 | async-start | bytes 1048576 | tf_op jit(solution)/shard_map/all_to_all | solution.py:225
  141.2 1.7 %collective-permute-start.13 = (f32[32,2048]{1,0:T(8,128)}, f32[32,2048]{1,0:T(8,128)S(1)}, u32[]{:S(2)}, u32[]{:S(2)}) collective-permute-start(f32[32,2048]{1,0:T(8,128)} %convolution_add_fusion), channel_id=1, source_target_pairs={{0,1},{1,0},{2,3},{3,2},{4,5},{5,4},{6,7},{7,6},{8,9},{9,8},{10,11... | collective-permute-start | bytes 786440 | tf_op jit(solution)/shard_map/ppermute | solution.py:103
Sparse Core Ops, SparseCore 0:
  10.7 57.7 all-gather.1
